TPU v7x, 32 devices: a whole 2x2x4 slice. The times are simulated.
32 devices in a mesh: kv: 16 (over z, x, core), tp: 2 (over y).
Axes of the slice: x: 2, y: 2, z: 4, core: 2. Of those that a mesh axis runs over, the one named last changes fastest.
Arguments:
- queries: bfloat16 [2048, 4096], P('kv', 'tp'), may hold values from -6 to 6
- keys: bfloat16 [2048, 512], P('kv', 'tp'), may hold values from -6 to 6
- values: bfloat16 [2048, 512], P('kv', 'tp'), may hold values from -6 to 6
- logsum: float32 [2048, 32], P('kv', 'tp'), may hold values from 2 to 6
- out_grad: bfloat16 [2048, 4096], P('kv', 'tp'), may hold values from -6 to 6
- normed_input: bfloat16 [2048, 4096], P('kv', 'tp'), may hold values from -6 to 6
- chosen: int32 [32, 16], P('kv'), may hold values from 0 to 63, as said below
Outputs:
- query_grad: float32 [2048, 4096], P('kv', 'tp')
- key_grad: float32 [2048, 512], P('kv', 'tp')
- value_grad: float32 [2048, 512], P('kv', 'tp')
- value_weight_grad: float32 [4096, 512], P('kv', 'tp')
Inputs may be any that keep to these rules, and one draw needn't show every extreme that they name: `chosen`: each row r names 16 distinct key blocks, among them block 0 and the blocks r * 2 to r * 2 + 64 / 32 - 1 that hold the query block's own positions. The rows of one device (aligned runs of 2 rows) name at most one block of any other device's 128 / 32 blocks. Blocks after the query block may be named; their keys are masked.
All inputs are finite; a program needn't handle non-finite values.
Results may differ from a plain program's by a relative error of at most 0.008.
Values may be sent and summed in bfloat16 or wider, within the bound.
A program may use at most 64 MiB of HBM per device.

v0:
```python
import functools

import jax
import jax.numpy as jnp
from jax import lax
from jax.experimental import pallas as pl
from jax.experimental.pallas import tpu as pltpu
from jax.sharding import PartitionSpec as P

HD = 128
QB = 64
KB = 32
NSEL = 16

MESH = pl.DeviceIdType.MESH
F32 = jnp.float32
BF16 = jnp.bfloat16


def remote(src, dst, send_sem, recv_sem, device_id):
    return pltpu.make_async_remote_copy(
        src_ref=src,
        dst_ref=dst,
        send_sem=send_sem,
        recv_sem=recv_sem,
        device_id=device_id,
        device_id_type=MESH,
    )


class Gather:
    def __init__(self, pool, send_z, send_x, send_c, recv, me, n, xs):
        self.pool, self.recv = pool, recv
        self.send_z, self.send_x, self.send_c = send_z, send_x, send_c
        self.me, self.n, self.xs = me, n, xs
        self.row = 2 * xs
        self.zs = n // self.row
        self.z = me // self.row
        self.r = me % self.row
        self.x = self.r // 2
        self.c = self.r % 2
        self.sends = self.zs - 1
        self.planes = self.zs

    def copy(self, slot, send_sem, dest):
        return remote(
            self.pool.at[slot], self.pool.at[slot], send_sem, self.recv.at[slot], {"kv": dest}
        )

    def plane(self, k):
        return (self.z - k + self.zs) % self.zs

    def along_z(self, k):
        dest = ((self.z + k) % self.zs) * self.row + self.r
        return self.copy(self.me, self.send_z.at[k], dest)

    def along_x(self, k, d):
        slot = self.plane(k) * self.row + self.r
        dest = self.z * self.row + ((self.x + d) % self.xs) * 2 + self.c
        return self.copy(slot, self.send_x.at[k, d], dest)

    def across(self, k, d):
        slot = self.plane(k) * self.row + ((self.x + d) % self.xs) * 2 + self.c
        dest = self.z * self.row + self.x * 2 + (1 - self.c)
        return self.copy(slot, self.send_c.at[k, d], dest)

    def wait_slot(self, slot):
        self.copy(slot, self.send_z.at[0], (self.me + 1) % self.n).wait_recv()

    def start(self):
        def body(k, _):
            self.along_z(k).start()
            return 0

        lax.fori_loop(1, self.sends + 1, body, 0)

    def relay(self):
        def step(k, first):
            slot = self.plane(k) * self.row + self.r
            if not first:
                self.wait_slot(slot)
            for d in range(1, self.xs):
                self.along_x(k, d).start()
            self.across(k, 0).start()

        def cross(k):
            for d in range(1, self.xs):
                slot = self.plane(k) * self.row + ((self.x + d) % self.xs) * 2 + self.c
                self.wait_slot(slot)
                self.across(k, d).start()

        step(0, True)

        def body(k, _):
            step(k, False)
            cross(k - 1)
            return 0

        lax.fori_loop(1, self.planes, body, 0)
        cross(self.planes - 1)

    def finish(self):
        def body(k, _):
            for d in range(self.xs):
                self.wait_slot(
                    self.plane(k) * self.row + ((self.x + d) % self.xs) * 2 + (1 - self.c)
                )
            return 0

        lax.fori_loop(0, self.planes, body, 0)

    def drain(self):
        def zbody(k, _):
            self.along_z(k).wait_send()
            return 0

        lax.fori_loop(1, self.sends + 1, zbody, 0)

        def body(k, _):
            for d in range(1, self.xs):
                self.along_x(k, d).wait_send()
            for d in range(self.xs):
                self.across(k, d).wait_send()
            return 0

        lax.fori_loop(0, self.planes, body, 0)


def dot(a, b, dims):
    return lax.dot_general(a, b, (dims, ((), ())), preferred_element_type=F32)


def kernel(
    n,
    tp,
    chosen,
    queries,
    keys,
    values,
    logsum,
    out_grad,
    normed,
    query_grad,
    key_grad,
    value_grad,
    weight_grad,
    pool,
    ask,
    asked,
    give,
    low_pool,
    norm_parts,
    norm_via,
    norm_pool,
    sel,
    s_buf,
    d_buf,
    p_low,
    ds_low,
    part,
    back,
    got,
    table,
    local_sem,
    ask_send,
    ask_recv,
    kv_send,
    kv_recv,
    back_send,
    back_recv,
    via_send,
    via_recv,
    norm_send,
    norm_recv,
    swap_send,
    swap_recv,
    lo_z,
    lo_x,
    lo_c,
    lo_recv,
):
    me = lax.axis_index("kv")
    col = lax.axis_index("tp")
    kblocks = keys.shape[0]
    tok = kblocks * KB
    qblocks = tok // QB
    kv_cols = keys.shape[2]
    kv_heads = kv_cols // HD
    group = queries.shape[1] // kv_cols
    per = n // tp
    sub = norm_parts.shape[2]
    rows = sub * tp
    scale = HD ** (-0.5)
    entries = qblocks * NSEL
    after = (me + 1) % n

    barrier = pltpu.get_barrier_semaphore()

    def greet(i, _):
        for t in range(tp):
            pl.semaphore_signal(
                barrier, inc=1, device_id={"kv": i, "tp": t}, device_id_type=MESH
            )
        return 0

    lax.fori_loop(0, n, greet, 0)
    own = []
    for w in range(kblocks):
        for a, ref in ((0, keys), (1, values)):
            c = pltpu.make_async_copy(ref.at[w], pool.at[n + w, a], local_sem.at[w, a])
            c.start()
            own.append(c)

    def look(i, _):
        block = jnp.int32(0)
        for b in range(qblocks):
            found = jnp.int32(entries)
            for e in range(NSEL):
                c = chosen[b, e]
                here = c // kblocks == i
                found = jnp.where(here, b * NSEL + e, found)
                block = jnp.where(here, c % kblocks + 1, block)
            table[b, i] = found
        ask[i] = jnp.full(ask.shape[1:], block, jnp.int32)
        return 0

    lax.fori_loop(0, me, look, 0)
    for m in range(normed.shape[1] // HD):
        turned = normed[:, m * HD : (m + 1) * HD].T
        for p in range(0, HD, sub):
            at = m * HD + p
            norm_parts[at % rows // sub, at // rows] = turned[p : p + sub]

    pl.semaphore_wait(barrier, n * tp)

    def ask_copy(i):
        return remote(ask.at[i], asked.at[me], ask_send.at[i], ask_recv.at[me], {"kv": i})

    def ask_start(i, _):
        ask_copy(i).start()
        return 0

    lax.fori_loop(0, me, ask_start, 0)

    def via_copy(d):
        q = (col + d) % tp
        return remote(
            norm_parts.at[q], norm_via.at[d], via_send.at[d], via_recv.at[d], {"tp": q}
        )

    for d in range(1, tp):
        via_copy(d).start()

    for w in range(kblocks):
        for b in range(qblocks):
            found = jnp.int32(entries)
            for e in range(NSEL):
                found = jnp.where(chosen[b, e] == me * kblocks + w, b * NSEL + e, found)
            table[b, n + w] = found
    part[:, entries] = jnp.zeros_like(part[:, entries])

    def kv_copy(j):
        return remote(give.at[j], pool.at[me], kv_send.at[j], kv_recv.at[me], {"kv": j})

    def answer(k, _):
        j = n - 1 - k
        remote(ask.at[0], asked.at[j], ask_send.at[0], ask_recv.at[j], {"kv": after}).wait_recv()
        named = asked[j]
        for a, ref in ((0, keys), (1, values)):
            block = jnp.zeros((KB, kv_cols), F32)
            for w in range(kblocks):
                mask = jnp.concatenate([named == w + 1] * (KB // 8), axis=0)
                block = jnp.where(mask, ref[w].astype(F32), block)
            give[j, a] = block.astype(BF16)
        kv_copy(j).start()
        return 0

    lax.fori_loop(0, n - 1 - me, answer, 0)

    def norm_each(act, act_local):
        def body(k0, _):
            for d in range(tp):
                t = (col + tp - d) % tp
                k = (k0 + me) % per
                dest = t * per + k
                src = norm_parts.at[col, k] if d == 0 else norm_via.at[d, k]

                @pl.when(dest == me)
                def _():
                    act_local(
                        pltpu.make_async_copy(src, norm_pool.at[col, me], norm_recv.at[me])
                    )

                @pl.when(dest != me)
                def _():
                    act(
                        remote(
                            src,
                            norm_pool.at[col, me],
                            norm_send.at[d, k],
                            norm_recv.at[me],
                            {"kv": dest},
                        )
                    )

            return 0

        lax.fori_loop(0, per, body, 0)

    for d in range(1, tp):
        via_copy(d).wait_recv()
    norm_each(lambda c: c.start(), lambda c: c.start())

    for c in own:
        c.wait()

    def kv_wait(j, _):
        remote(give.at[0], pool.at[j], kv_send.at[0], kv_recv.at[j], {"kv": after}).wait_recv()
        return 0

    lax.fori_loop(0, me, kv_wait, 0)
    span = NSEL * KB
    width = group * QB
    key_iota = lax.broadcasted_iota(jnp.int32, (KB, width), 0)
    row_iota = lax.broadcasted_iota(jnp.int32, (KB, width), 1) % QB
    logs = logsum[...].T
    for b in range(qblocks):
        for e in range(NSEL):
            block = chosen[b, e]
            owner = block // kblocks
            slot = jnp.where(owner == me, n + block % kblocks, jnp.where(owner < me, owner, n))
            for a in range(2):
                sel[a, e * KB : (e + 1) * KB, :] = pool[slot, a]
        for g in range(kv_heads):
            lanes = slice(g * HD, (g + 1) * HD)

            def stack(ref):
                return jnp.concatenate(
                    [
                        ref[b * QB : (b + 1) * QB, (g * group + h) * HD : (g * group + h + 1) * HD]
                        for h in range(group)
                    ],
                    axis=0,
                )

            q = stack(queries)
            do = stack(out_grad)
            k_sel = sel[0, :, lanes]
            s_buf[...] = dot(k_sel, q, ((1,), (1,)))
            d_buf[...] = dot(sel[1, :, lanes], do, ((1,), (1,)))
            log = jnp.concatenate(
                [
                    logs[g * group + h : g * group + h + 1, b * QB : (b + 1) * QB]
                    for h in range(group)
                ],
                axis=1,
            )
            delta = jnp.zeros((8, width), F32)
            for e in range(NSEL):
                at = slice(e * KB, (e + 1) * KB)
                limit = (me * tok + b * QB) - chosen[b, e] * KB
                valid = key_iota - row_iota <= limit
                p = jnp.where(valid, jnp.exp(s_buf[at, :] * scale - log), 0.0)
                s_buf[at, :] = p
                p_low[at, :] = p.astype(BF16)
                pd = p * d_buf[at, :]
                delta = delta + jnp.sum(pd.reshape(KB // 8, 8, width), axis=0)
            delta = jnp.sum(delta, axis=0, keepdims=True)
            for e in range(NSEL):
                at = slice(e * KB, (e + 1) * KB)
                ds_low[at, :] = (s_buf[at, :] * (d_buf[at, :] - delta)).astype(BF16)
            ds = ds_low[...]
            here = slice(b * NSEL, (b + 1) * NSEL)
            part[0, here, :, lanes] = (dot(ds, q, ((1,), (0,))) * scale).reshape(NSEL, KB, HD)
            part[1, here, :, lanes] = dot(p_low[...], do, ((1,), (0,))).reshape(NSEL, KB, HD)
            dq = dot(ds, k_sel, ((0,), (0,))) * scale
            for h in range(group):
                query_grad[
                    b * QB : (b + 1) * QB, (g * group + h) * HD : (g * group + h + 1) * HD
                ] = dq[h * QB : (h + 1) * QB]

    def back_copy(i):
        return remote(back.at[i], got.at[me], back_send.at[i], back_recv.at[me], {"kv": i})

    def send_back(i, _):
        for a in range(2):
            total = part[a, table[0, i]]
            for b in range(1, qblocks):
                total = total + part[a, table[b, i]]
            back[i, a] = total.astype(BF16)
        back_copy(i).start()
        return 0

    lax.fori_loop(0, me, send_back, 0)

    for w in range(kblocks):
        for a, out in ((0, key_grad), (1, value_grad)):
            total = part[a, table[0, n + w]]
            for b in range(1, qblocks):
                total = total + part[a, table[b, n + w]]
            out[w] = total

    def swap_copy(d):
        q = (col + d) % tp
        return remote(
            norm_pool.at[col], norm_pool.at[col], swap_send.at[d], swap_recv.at[d], {"tp": q}
        )

    def norm_wait(j, _):
        pltpu.make_async_copy(
            norm_pool.at[col, j], norm_pool.at[col, j], norm_recv.at[j]
        ).wait()
        return 0

    lax.fori_loop(0, n, norm_wait, 0)
    for d in range(1, tp):
        swap_copy(d).start()

    def add_back(j, _):
        remote(
            back.at[0], got.at[j], back_send.at[0], back_recv.at[j], {"kv": after}
        ).wait_recv()
        named = asked[j]
        terms = [got[j, a].astype(F32) for a in range(2)]
        for w in range(kblocks):
            mask = jnp.concatenate([named == w + 1] * (KB // 8), axis=0)
            for a, out in ((0, key_grad), (1, value_grad)):
                out[w] += jnp.where(mask, terms[a], 0.0)
        return 0

    lax.fori_loop(me + 1, n, add_back, 0)

    low_pool[me] = value_grad[...].reshape(tok, kv_cols).astype(BF16)
    low = Gather(low_pool, lo_z, lo_x, lo_c, lo_recv, me, n, tp)
    low.start()
    low.relay()
    for d in range(1, tp):
        q = (col + tp - d) % tp
        remote(
            norm_pool.at[q], norm_pool.at[q], swap_send.at[d], swap_recv.at[d], {"tp": q}
        ).wait_recv()
    low.finish()

    row = low.row

    def product(z, q):
        a = jnp.concatenate([norm_pool[q, z * row + i] for i in range(row)], axis=1)
        v = jnp.concatenate([low_pool[z * row + i] for i in range(row)], axis=0)
        return dot(a, v, ((1,), (0,)))

    for q in range(tp):
        weight_grad[q * sub : (q + 1) * sub] = product(0, q)

    def weigh(z, _):
        for q in range(tp):
            weight_grad[q * sub : (q + 1) * sub] += product(z, q)
        return 0

    lax.fori_loop(1, low.zs, weigh, 0)

    low.drain()

    def drain_early(i, _):
        ask_copy(i).wait_send()
        back_copy(i).wait_send()
        return 0

    lax.fori_loop(0, me, drain_early, 0)

    def drain_late(j, _):
        kv_copy(j).wait_send()
        return 0

    lax.fori_loop(me + 1, n, drain_late, 0)
    for d in range(1, tp):
        via_copy(d).wait_send()
        swap_copy(d).wait_send()
    norm_each(lambda c: c.wait_send(), lambda c: None)


def local(n, tp, queries, keys, values, logsum, out_grad, normed_input, chosen):
    tok, kv_cols = keys.shape
    kv_heads = kv_cols // HD
    group = queries.shape[1] // kv_cols
    kblocks = tok // KB
    qblocks = tok // QB
    rows = normed_input.shape[1] * tp // n
    zs = n // (2 * tp)
    entries = qblocks * NSEL
    span = NSEL * KB
    width = group * QB
    per = n // tp
    vmem = pl.BlockSpec(memory_space=pltpu.VMEM)
    dma = pltpu.SemaphoreType.DMA
    outs = pl.pallas_call(
        functools.partial(kernel, n, tp),
        out_shape=(
            jax.ShapeDtypeStruct((tok, queries.shape[1]), F32),
            jax.ShapeDtypeStruct((kblocks, KB, kv_cols), F32),
            jax.ShapeDtypeStruct((kblocks, KB, kv_cols), F32),
            jax.ShapeDtypeStruct((rows, kv_cols), F32),
        ),
        in_specs=[pl.BlockSpec(memory_space=pltpu.SMEM)] + [vmem] * 6,
        out_specs=(vmem,) * 4,
        scratch_shapes=[
            pltpu.VMEM((n + kblocks, 2, KB, kv_cols), BF16),
            pltpu.VMEM((n, 8, kv_cols), jnp.int32),
            pltpu.VMEM((n, 8, kv_cols), jnp.int32),
            pltpu.VMEM((n, 2, KB, kv_cols), BF16),
            pltpu.VMEM((n, tok, kv_cols), BF16),
            pltpu.VMEM((tp, per, rows // tp, tok), BF16),
            pltpu.VMEM((tp, per, rows // tp, tok), BF16),
            pltpu.VMEM((tp, n, rows // tp, tok), BF16),
            pltpu.VMEM((2, span, kv_cols), BF16),
            pltpu.VMEM((span, width), F32),
            pltpu.VMEM((span, width), F32),
            pltpu.VMEM((span, width), BF16),
            pltpu.VMEM((span, width), BF16),
            pltpu.VMEM((2, entries + 1, KB, kv_cols), F32),
            pltpu.VMEM((n, 2, KB, kv_cols), BF16),
            pltpu.VMEM((n, 2, KB, kv_cols), BF16),
            pltpu.SMEM((qblocks, n + kblocks), jnp.int32),
            dma((kblocks, 2)),
            dma((n,)),
            dma((n,)),
            dma((n,)),
            dma((n,)),
            dma((n,)),
            dma((n,)),
            dma((tp,)),
            dma((tp,)),
            dma((tp, per)),
            dma((n,)),
            dma((tp,)),
            dma((tp,)),
            dma((zs,)),
            dma((zs, tp)),
            dma((zs, tp)),
            dma((n,)),
        ],
        compiler_params=pltpu.CompilerParams(
            collective_id=0, has_side_effects=True, vmem_limit_bytes=60 * 1024 * 1024
        ),
        name="attention_back",
    )(
        chosen,
        queries,
        keys.reshape(kblocks, KB, kv_cols),
        values.reshape(kblocks, KB, kv_cols),
        logsum,
        out_grad,
        normed_input,
    )
    query_grad, key_grad, value_grad, weight_grad = outs
    return (
        query_grad,
        key_grad.reshape(tok, kv_cols),
        value_grad.reshape(tok, kv_cols),
        weight_grad,
    )


def solution(mesh):
    n, tp = mesh.shape["kv"], mesh.shape["tp"]
    in_specs = (P("kv", "tp"),) * 6 + (P("kv", None),)
    out_specs = (P("kv", "tp"),) * 4
    return jax.shard_map(
        functools.partial(local, n, tp),
        mesh=mesh,
        in_specs=in_specs,
        out_specs=out_specs,
        check_vma=False,
    )
```

profile of v0, /device:TPU:23, one launch (start us, length us, event | category | flops | bytes accessed | tf_op | source)
XLA Modules:
  0.0 65.5 jit_solution(7148925575105676344)
XLA Ops:
  0.6 1.4 %copy.11.logsum = f32[128,16]{1,0:T(8,128)} copy(f32[128,16]{0,1:T(8,128)} %param.10) | data formatting | bytes 16384 | tf_op args[3]
  2.1 59.0 %attention_back.1 = (f32[128,2048]{1,0:T(8,128)}, f32[4,32,256]{2,1,0:T(8,128)}, f32[4,32,256]{2,1,0:T(8,128)}, f32[256,256]{1,0:T(8,128)}) custom-call(s32[2,16]{1,0:T(2,128)} %chosen.1, bf16[128,2048]{1,0:T(8,128)(2,1)} %queries.1, bf16[4,32,256]{2,1,0:T(8,128)(2,1)} %bitcast.6, bf16[4,32,256]{2,1,0:T(8,128)(2,1)} %bitcast.7, f32[128,16]{1,0:T(8,128)} %copy.11.logsum, ...), custom_call_target="tpu_custom_call" | custom-call | tf_op jit(solution)/shard_map/attention_back/pallas_call | solution.py:495
  61.1 0.0 copy-start.2
  61.1 0.0 copy-start.1
  61.1 2.3 %copy.16 = f32[128,2048]{1,0:T(8,128)} copy(f32[128,2048]{1,0:T(8,128)} %get-tuple-element.16) | data formatting | bytes 2097152
  63.5 0.0 copy-done.2
  63.5 0.0 copy-start
  63.5 0.7 %copy.17 = f32[128,256]{1,0:T(8,128)} copy(f32[128,256]{1,0:T(8,128)S(1)} %bitcast.5) | data formatting | bytes 262144
  64.1 0.0 copy-done.1
  64.1 0.7 %copy.18 = f32[128,256]{1,0:T(8,128)} copy(f32[128,256]{1,0:T(8,128)S(1)} %bitcast.4) | data formatting | bytes 262144
  64.8 0.0 copy-done
  64.8 0.7 %copy.19 = f32[256,256]{1,0:T(8,128)} copy(f32[256,256]{1,0:T(8,128)S(1)} %copy-done) | data formatting | bytes 524288
Async XLA Ops:
  61.1 2.4 %copy-start.2 = (f32[4,32,256]{2,1,0:T(8,128)S(1)}, f32[4,32,256]{2,1,0:T(8,128)}, u32[]{:S(2)}) copy-start(f32[4,32,256]{2,1,0:T(8,128)} %get-tuple-element.9) | copy-start | bytes 393220
  61.1 3.0 %copy-start.1 = (f32[4,32,256]{2,1,0:T(8,128)S(1)}, f32[4,32,256]{2,1,0:T(8,128)}, u32[]{:S(2)}) copy-start(f32[4,32,256]{2,1,0:T(8,128)} %get-tuple-element.10) | copy-start | bytes 393220
  63.5 1.3 %copy-start = (f32[256,256]{1,0:T(8,128)S(1)}, f32[256,256]{1,0:T(8,128)}, u32[]{:S(2)}) copy-start(f32[256,256]{1,0:T(8,128)} %get-tuple-element.19) | copy-start | bytes 786436
where the time goes:
time: 65.7 us; the launch traced here: 65.5 us
  Pallas kernels  59 us (90%)
  local copies, waits for them, and re-layouts  5.79 us (9%)
  between operations  0.66 us (1%)
    pallas_call x1, Pallas kernels, local(): pl.pallas_call(functools.partial(kernel, n, tp), out_shape=(jax.ShapeDtyp...  59 us
    unnamed x11, local copies, waits for them, and re-layouts  5.79 us

commit v1 on v0

v1 whole, which is shorter than its diff:
```python
import functools

import jax
import jax.numpy as jnp
from jax import lax
from jax.experimental import pallas as pl
from jax.experimental.pallas import tpu as pltpu
from jax.sharding import PartitionSpec as P

HD = 128
QB = 64
KB = 32
NSEL = 16
FAR = 1e30
LOG2E = 1.4426950408889634

MESH = pl.DeviceIdType.MESH
F32 = jnp.float32
BF16 = jnp.bfloat16


def remote(src, dst, send_sem, recv_sem, device_id):
    return pltpu.make_async_remote_copy(
        src_ref=src,
        dst_ref=dst,
        send_sem=send_sem,
        recv_sem=recv_sem,
        device_id=device_id,
        device_id_type=MESH,
    )


def dot(a, b, dims):
    return lax.dot_general(a, b, (dims, ((), ())), preferred_element_type=F32)


def loop(first, last, body):
    def step(i, carry):
        body(i)
        return carry

    lax.fori_loop(first, last, step, 0)


def mark(name):
    pass


def kernel(
    n,
    tp,
    chosen_hbm,
    queries,
    keys,
    values,
    logsum,
    out_grad,
    normed_hbm,
    query_grad,
    key_grad,
    value_grad,
    weight_grad,
    chosen,
    q_all,
    do_all,
    logs,
    log2s,
    normed,
    pool,
    ask,
    asked,
    named,
    give,
    back_v,
    back_k,
    got_v,
    got_k,
    low_pool,
    norm_parts,
    norm_via,
    norm_pool,
    pen,
    pen_own,
    s_buf,
    dp,
    p_low,
    delta,
    dq_acc,
    in_sem,
    ask_send,
    ask_recv,
    out_send,
    kv_recv,
    bv_recv,
    bk_recv,
    via_send,
    via_recv,
    norm_send,
    norm_recv,
    swap_send,
    swap_recv,
    lo_send,
    lo_recv,
):
    me = lax.axis_index("kv")
    col = lax.axis_index("tp")
    kblocks = keys.shape[0]
    tok = kblocks * KB
    qblocks = tok // QB
    kv_cols = keys.shape[2]
    kv_heads = kv_cols // HD
    group = queries.shape[1] // kv_cols
    width = group * tok
    per = n // tp
    sub = norm_parts.shape[2]
    rows = sub * tp
    scale = HD ** (-0.5)
    xs = tp
    row = 2 * xs
    zs = n // row
    z = me // row
    r = me % row
    x = r // 2
    c = r % 2
    lanes = [slice(g * HD, (g + 1) * HD) for g in range(kv_heads)]

    barrier = pltpu.get_barrier_semaphore()

    mark("greet")

    def greet(i):
        pl.semaphore_signal(barrier, inc=1, device_id={"kv": i}, device_id_type=MESH)

    loop(0, n, greet)
    for d in range(1, tp):
        pl.semaphore_signal(
            barrier, inc=1, device_id={"tp": (col + d) % tp}, device_id_type=MESH
        )

    ins = [
        [pltpu.make_async_copy(chosen_hbm, chosen, in_sem.at[0])],
        [pltpu.make_async_copy(normed_hbm, normed, in_sem.at[1])],
        [
            pltpu.make_async_copy(ref, pool.at[pl.ds(n, kblocks), a], in_sem.at[2 + a])
            for a, ref in ((0, keys), (1, values))
        ],
        [pltpu.make_async_copy(logsum, logs, in_sem.at[4])],
    ]
    big = []
    for a, (src, dst) in enumerate(((queries, q_all), (out_grad, do_all))):
        for g in range(kv_heads):
            for h in range(group):
                at = (g * group + h) * HD
                big.append(
                    pltpu.make_async_copy(
                        src.at[:, at : at + HD],
                        dst.at[g, h * tok : (h + 1) * tok],
                        in_sem.at[5 + a],
                    )
                )
    for cs in ins:
        for cp in cs:
            cp.start()
    for cp in big:
        cp.start()

    mark("ask")
    for q in range(row):

        @pl.when(q >= r)
        def _():
            pool[z * row + q] = jnp.zeros_like(pool[z * row + q])

    ins[0][0].wait()
    lane = lax.broadcasted_iota(jnp.int32, (8, HD), 1)
    base = lane * kblocks
    wanted = jnp.zeros((8, HD), F32)
    missing = []
    missing_own = []
    for b in range(qblocks):
        far = jnp.full((8, HD), FAR, F32)
        far_own = jnp.full((8, HD), FAR, F32)
        for e in range(NSEL):
            block = chosen[b, e]
            at = block - base
            hit = (at >= 0) & (at < kblocks)
            wanted = jnp.where(hit, (at + 1).astype(F32), wanted)
            far = jnp.where(hit, 0.0, far)
            far_own = jnp.where(block - me * kblocks == lane, 0.0, far_own)
        missing.append(jnp.broadcast_to(far[:1], (QB, HD)))
        missing_own.append(jnp.broadcast_to(far_own[:1], (QB, HD)))
    ask[...] = wanted
    pen[...] = jnp.concatenate(missing, axis=0).T
    pen_own[...] = jnp.concatenate(missing_own, axis=0).T

    mark("turn")
    ins[1][0].wait()
    for m in range(normed.shape[1] // HD):
        turned = normed[:, m * HD : (m + 1) * HD].T
        for p in range(0, HD, sub):
            at = m * HD + p
            norm_parts[at % rows // sub, at // rows] = turned[p : p + sub]

    mark("barrier")
    pl.semaphore_wait(barrier, n + tp - 1)

    def place(i):
        return jnp.where(i // row == z, zs + i % row, i // row)

    mark("asksend")

    def ask_copy(i):
        return remote(ask, asked.at[me], ask_send.at[i], ask_recv.at[place_of_me(i)], {"kv": i})

    def place_of_me(i):
        return jnp.where(i // row == z, zs + r, z)

    loop(0, me, lambda i: ask_copy(i).start())

    def via_copy(d, k):
        q = (col + d) % tp
        return remote(
            norm_parts.at[q, k], norm_via.at[d, k], via_send.at[d], via_recv.at[d, k], {"tp": q}
        )

    for d in range(1, tp):
        loop(0, per, lambda k: via_copy(d, k).start())

    def norm_copy(d, k):
        t = (col + tp - d) % tp
        dest = t * per + k
        src = norm_parts.at[col, k] if d == 0 else norm_via.at[d, k]
        return remote(
            src, norm_pool.at[col, me], norm_send.at[0], norm_recv.at[place_of_me(dest)],
            {"kv": dest},
        )

    def norm_start(d, k, low):
        t = (col + tp - d) % tp
        dest = t * per + k

        if low:

            @pl.when(dest == me)
            def _():
                src = norm_parts[col, k] if d == 0 else norm_via[d, k]
                norm_pool[col, me] = src

            @pl.when((dest != me) & (dest // row <= z))
            def _():
                norm_copy(d, k).start()
        else:

            @pl.when(dest // row > z)
            def _():
                norm_copy(d, k).start()

    mark("normlow")
    loop(0, per, lambda k: norm_start(0, k, True))

    mark("own")
    for cp in ins[2] + ins[3]:
        cp.wait()
    for cp in big:
        cp.wait()
    for g in range(kv_heads):
        log2s[g] = jnp.concatenate(
            [logs[g * group + h : g * group + h + 1] * LOG2E for h in range(group)], axis=1
        )

    def take(a, first, count, g):
        return pool[pl.ds(first, count), a, :, lanes[g]].reshape(count * KB, HD)

    key_iota = lax.broadcasted_iota(jnp.int32, (KB, tok), 0)
    row_iota = lax.broadcasted_iota(jnp.int32, (KB, tok), 1)

    def early(first, count, own):
        for g in range(kv_heads):
            s_buf[: count * KB] = dot(take(0, first, count, g), q_all[g], ((1,), (1,)))
            dp[g, pl.ds(first, count)] = dot(
                take(1, first, count, g), do_all[g], ((1,), (1,))
            ).reshape(count, KB, width)
            total = jnp.zeros((8, width), F32) if own else delta[g]
            for u in range(count):
                if own:
                    gone = jnp.where(key_iota + u * KB <= row_iota, 0.0, FAR)
                    gone = gone + pen_own[u : u + 1]
                else:
                    gone = pen[pl.ds(first + u, 1)]
                bias = log2s[g] + jnp.concatenate([gone] * group, axis=1)
                p = jnp.exp2(s_buf[u * KB : (u + 1) * KB] * (scale * LOG2E) - bias)
                p_low[g, first + u] = p.astype(BF16)
                pd = p * dp[g, first + u]
                total = total + jnp.sum(pd.reshape(KB // 8, 8, width), axis=0)
            delta[g] = total
            dv = dot(
                p_low[g, pl.ds(first, count)].reshape(count * KB, width), do_all[g], ((1,), (0,))
            ).reshape(count, KB, HD)
            if own:
                value_grad[:, :, lanes[g]] = dv
            else:
                back_v[pl.ds(first, count), :, lanes[g]] = dv.astype(BF16)

    early(n, kblocks, True)

    mark("answer")

    def name(j):
        mine = jnp.where(lane == me, asked[j], 0.0)
        named[j] = jnp.broadcast_to(jnp.sum(mine, axis=1, keepdims=True), (8, kv_cols))

    def masks(j):
        return [
            jnp.concatenate([named[j] == w + 1.0] * (KB // 8), axis=0) for w in range(kblocks)
        ]

    def kv_copy(j):
        return remote(
            give.at[j], pool.at[me], out_send.at[0], kv_recv.at[place_of_me(j)], {"kv": j}
        )

    def answer(j):
        name(j)
        hit = masks(j)
        for a in range(2):
            block = jnp.zeros((KB, kv_cols), F32)
            for w in range(kblocks):
                block = jnp.where(hit[w], pool[n + w, a].astype(F32), block)
            give[j, a] = block.astype(BF16)
        kv_copy(j).start()

    def wait_plane(ref, sem, k):
        at = ref.at[pl.ds(k * row, row)]
        pltpu.make_async_copy(at, at, sem.at[k]).wait()

    def wait_peer(ref, sem, q):
        at = ref.at[z * row + q]
        pltpu.make_async_copy(at, at, sem.at[zs + q]).wait()

    def answer_plane(i):
        k = zs - 1 - i
        wait_plane(asked, ask_recv, k)
        loop(0, row, lambda q: answer(k * row + q))

    loop(0, zs - 1 - z, answer_plane)
    for q in reversed(range(1, row)):

        @pl.when(q > r)
        def _():
            wait_peer(asked, ask_recv, q)
            answer(z * row + q)

    mark("norm")
    for d in range(1, tp):

        def forward(k):
            at = norm_via.at[d, k]
            pltpu.make_async_copy(at, at, via_recv.at[d, k]).wait()
            norm_start(d, k, True)

        loop(0, per, forward)
    for d in range(tp):
        loop(0, per, lambda k: norm_start(d, k, False))

    mark("near")

    def bv_copy(i):
        return remote(
            back_v.at[i], got_v.at[me], out_send.at[0], bv_recv.at[place_of_me(i)], {"kv": i}
        )

    def bk_copy(i):
        return remote(
            back_k.at[i], got_k.at[me], out_send.at[0], bk_recv.at[place_of_me(i)], {"kv": i}
        )

    def peers(act, test):
        for q in range(row):

            @pl.when(test(q))
            def _():
                act(q)

    peers(lambda q: wait_peer(pool, kv_recv, q), lambda q: q < r)
    early(z * row, row, False)
    peers(lambda q: bv_copy(z * row + q).start(), lambda q: q < r)

    mark("far")

    def early_plane(i):
        k = z - 1 - i
        wait_plane(pool, kv_recv, k)
        early(k * row, row, False)
        loop(0, row, lambda q: bv_copy(k * row + q).start())

    loop(0, z, early_plane)

    mark("late")
    for g in range(kv_heads):
        delta[g] = jnp.broadcast_to(jnp.sum(delta[g], axis=0, keepdims=True), (8, width))

    def late(first, count, own):
        for g in range(kv_heads):
            for u in range(count):
                ds = p_low[g, first + u].astype(F32) * (dp[g, first + u] - delta[g, :1])
                p_low[g, first + u] = ds.astype(BF16)
            ds = p_low[g, pl.ds(first, count)].reshape(count * KB, width)
            dk = dot(ds, q_all[g], ((1,), (0,))).reshape(count, KB, HD) * scale
            if own:
                key_grad[:, :, lanes[g]] = dk
            else:
                back_k[pl.ds(first, count), :, lanes[g]] = dk.astype(BF16)
            dq = dot(take(0, first, count, g), ds, ((0,), (0,)))
            dq_acc[g] = dq if own else dq_acc[g] + dq

    late(n, kblocks, True)

    def late_plane(i):
        k = z - 1 - i
        late(k * row, row, False)
        loop(0, row, lambda q: bk_copy(k * row + q).start())

    loop(0, z, late_plane)
    late(z * row, row, False)
    peers(lambda q: bk_copy(z * row + q).start(), lambda q: q < r)

    mark("dq")
    for g in range(kv_heads):
        for h in range(group):
            at = (g * group + h) * HD
            query_grad[:, at : at + HD] = dq_acc[g, :, h * tok : (h + 1) * tok].T * scale

    def swap_copy(d, k):
        at = norm_pool.at[col, pl.ds(k * row, row)]
        return remote(at, at, swap_send.at[d], swap_recv.at[d, k], {"tp": (col + d) % tp})

    def swap(k):
        for d in range(1, tp):
            swap_copy(d, k).start()

    def swap_plane(k):
        wait_plane(norm_pool.at[col], norm_recv, k)
        swap(k)

    mark("swap1")
    peers(lambda q: wait_peer(norm_pool.at[col], norm_recv, q), lambda q: q != r)
    swap(z)
    loop(z + 1, zs, swap_plane)

    mark("addv")

    def add(j, got, out):
        hit = masks(j)
        term = got[j].astype(F32)
        for w in range(kblocks):
            out[w] += jnp.where(hit[w], term, 0.0)

    def add_all(got, sem, out):
        def one(q):
            wait_peer(got, sem, q)
            add(z * row + q, got, out)

        peers(one, lambda q: q > r)

        def plane(k):
            wait_plane(got, sem, k)
            loop(0, row, lambda q: add(k * row + q, got, out))

        loop(z + 1, zs, plane)

    add_all(got_v, bv_recv, value_grad)
    low_pool[me] = value_grad[...].reshape(tok, kv_cols).astype(BF16)

    mark("lowstart")

    def low_copy(slot, send, dest):
        return remote(
            low_pool.at[slot], low_pool.at[slot], lo_send.at[send], lo_recv.at[slot], {"kv": dest}
        )

    def low_wait(slot):
        at = low_pool.at[slot]
        pltpu.make_async_copy(at, at, lo_recv.at[slot]).wait()

    def plane_of(k):
        return (z - k + zs) % zs

    loop(1, zs, lambda k: low_copy(me, 0, (z + k) % zs * row + r).start())

    mark("swap2")
    loop(0, z, swap_plane)

    mark("lowrelay")

    def slot_of(k, d, core):
        return plane_of(k) * row + (x + d) % xs * 2 + core

    def across(k, d):
        low_copy(slot_of(k, d, c), 2, z * row + x * 2 + 1 - c).start()

    def relay(k, first):
        if not first:
            low_wait(slot_of(k, 0, c))
        for d in range(1, xs):
            low_copy(slot_of(k, 0, c), 1, z * row + (x + d) % xs * 2 + c).start()
        across(k, 0)

    def cross(k):
        for d in range(1, xs):
            low_wait(slot_of(k, d, c))
            across(k, d)

    def relay_next(k):
        relay(k, False)
        cross(k - 1)

    relay(0, True)
    loop(1, zs, relay_next)
    cross(zs - 1)

    mark("addk")
    add_all(got_k, bk_recv, key_grad)

    mark("product")

    def product(k, first):
        p = plane_of(k)
        for d in range(xs):
            low_wait(slot_of(k, d, 1 - c))
        for d in range(1, tp):
            q = (col + tp - d) % tp
            at = norm_pool.at[q, pl.ds(p * row, row)]
            pltpu.make_async_copy(at, at, swap_recv.at[d, p]).wait()
        v = low_pool[pl.ds(p * row, row)].reshape(row * tok, kv_cols)
        for q in range(tp):
            a = jnp.concatenate([norm_pool[q, p * row + i] for i in range(row)], axis=1)
            w = dot(a, v, ((1,), (0,)))
            if first:
                weight_grad[q * sub : (q + 1) * sub] = w
            else:
                weight_grad[q * sub : (q + 1) * sub] += w

    product(0, True)
    loop(1, zs, lambda k: product(k, False))

    mark("drain")

    def drain(ref, sem):
        pltpu.make_async_copy(ref, ref, sem).wait()

    drain(low_pool.at[pl.ds(0, zs - 1)], lo_send.at[0])
    drain(low_pool.at[pl.ds(0, zs * (xs - 1))], lo_send.at[1])
    drain(low_pool.at[pl.ds(0, zs * xs)], lo_send.at[2])
    drain(give.at[pl.ds(0, n - 1)], out_send.at[0])
    drain(norm_pool.at[0, pl.ds(0, n - 1)], norm_send.at[0])
    for d in range(1, tp):
        drain(norm_parts.at[0], via_send.at[d])
        drain(norm_pool.at[0], swap_send.at[d])
    loop(0, me, lambda i: ask_copy(i).wait_send())
    mark(None)


def finish(*refs):
    count = len(refs) // 2
    sem = refs[-1]
    copies = [
        pltpu.make_async_copy(refs[i], refs[count + i], sem.at[i]) for i in range(count)
    ]
    for cp in copies:
        cp.start()
    for cp in copies:
        cp.wait()


def local(n, tp, queries, keys, values, logsum, out_grad, normed_input, chosen):
    tok, kv_cols = keys.shape
    kv_heads = kv_cols // HD
    heads = queries.shape[1] // HD
    group = heads // kv_heads
    kblocks = tok // KB
    rows = normed_input.shape[1] * tp // n
    row = 2 * tp
    zs = n // row
    width = group * tok
    per = n // tp
    sub = rows // tp
    slots = n + kblocks
    hbm = pl.BlockSpec(memory_space=pltpu.HBM)
    vmem = pl.BlockSpec(memory_space=pltpu.VMEM)
    dma = pltpu.SemaphoreType.DMA
    groups = zs + row
    outs = (
        (tok, queries.shape[1]),
        (kblocks, KB, kv_cols),
        (kblocks, KB, kv_cols),
        (rows, kv_cols),
    )
    held = pl.pallas_call(
        functools.partial(kernel, n, tp),
        out_shape=tuple(pltpu.VMEM(shape, F32) for shape in outs),
        in_specs=[hbm] * 7,
        out_specs=(vmem,) * 4,
        scratch_shapes=[
            pltpu.SMEM(chosen.shape, jnp.int32),
            pltpu.VMEM((kv_heads, width, HD), BF16),
            pltpu.VMEM((kv_heads, width, HD), BF16),
            pltpu.VMEM((heads, tok), F32),
            pltpu.VMEM((kv_heads, 1, width), F32),
            pltpu.VMEM(normed_input.shape, BF16),
            pltpu.VMEM((slots, 2, KB, kv_cols), BF16),
            pltpu.VMEM((8, HD), F32),
            pltpu.VMEM((n, 8, HD), F32),
            pltpu.VMEM((n, 8, kv_cols), F32),
            pltpu.VMEM((n, 2, KB, kv_cols), BF16),
            pltpu.VMEM((n, KB, kv_cols), BF16),
            pltpu.VMEM((n, KB, kv_cols), BF16),
            pltpu.VMEM((n, KB, kv_cols), BF16),
            pltpu.VMEM((n, KB, kv_cols), BF16),
            pltpu.VMEM((n, tok, kv_cols), BF16),
            pltpu.VMEM((tp, per, sub, tok), BF16),
            pltpu.VMEM((tp, per, sub, tok), BF16),
            pltpu.VMEM((tp, n, sub, tok), BF16),
            pltpu.VMEM((HD, tok), F32),
            pltpu.VMEM((HD, tok), F32),
            pltpu.VMEM((max(row, kblocks) * KB, width), F32),
            pltpu.VMEM((kv_heads, slots, KB, width), F32),
            pltpu.VMEM((kv_heads, slots, KB, width), BF16),
            pltpu.VMEM((kv_heads, 8, width), F32),
            pltpu.VMEM((kv_heads, HD, width), F32),
            dma((7,)),
            dma((n,)),
            dma((groups,)),
            dma((1,)),
            dma((groups,)),
            dma((groups,)),
            dma((groups,)),
            dma((tp,)),
            dma((tp, per)),
            dma((1,)),
            dma((groups,)),
            dma((tp,)),
            dma((tp, zs)),
            dma((3,)),
            dma((n,)),
        ],
        compiler_params=pltpu.CompilerParams(
            collective_id=0, has_side_effects=True, vmem_limit_bytes=56 * 1024 * 1024
        ),
        name="attention_back",
    )(
        chosen,
        queries,
        keys.reshape(kblocks, KB, kv_cols),
        values.reshape(kblocks, KB, kv_cols),
        logsum.T,
        out_grad,
        normed_input,
    )
    query_grad, key_grad, value_grad, weight_grad = pl.pallas_call(
        finish,
        out_shape=tuple(jax.ShapeDtypeStruct(shape, F32) for shape in outs),
        in_specs=[vmem] * 4,
        out_specs=(hbm,) * 4,
        scratch_shapes=[dma((4,))],
        compiler_params=pltpu.CompilerParams(vmem_limit_bytes=4 * 1024 * 1024),
        name="write_out",
    )(*held)
    return (
        query_grad,
        key_grad.reshape(tok, kv_cols),
        value_grad.reshape(tok, kv_cols),
        weight_grad,
    )


def solution(mesh):
    n, tp = mesh.shape["kv"], mesh.shape["tp"]
    in_specs = (P("kv", "tp"),) * 6 + (P("kv", None),)
    out_specs = (P("kv", "tp"),) * 4
    return jax.shard_map(
        functools.partial(local, n, tp),
        mesh=mesh,
        in_specs=in_specs,
        out_specs=out_specs,
        check_vma=False,
    )
```

time: 65.7 us -> 49.7 us (0.76)
  the two profiles are of different devices: /device:TPU:23 before, /device:TPU:0 now
where the time goes in v1:
time: 49.7 us; the launch traced here: 49 us
  Pallas kernels  48.4 us (97%)
  between operations  0.64 us (1%)
    pallas_call x1, Pallas kernels, local(): pl.pallas_call(functools.partial(kernel, n, tp), out_shape=tuple((pltpu.V...  47.2 us
    pallas_call x1, Pallas kernels, local(): pl.pallas_call(finish, out_shape=tuple((jax.ShapeDtypeStruct(shape, F32)...  1.17 us

profile of v1, /device:TPU:0, one launch (start us, length us, event | category | flops | bytes accessed | tf_op | source)
XLA Modules:
  0.0 49.0 jit_solution(14292559754467431419)
XLA Ops:
  0.6 47.2 %attention_back.1 = (f32[128,2048]{1,0:T(8,128)S(1)}, f32[4,32,256]{2,1,0:T(8,128)S(1)}, f32[4,32,256]{2,1,0:T(8,128)S(1)}, f32[256,256]{1,0:T(8,128)S(1)}) custom-call(s32[2,16]{1,0:T(2,128)} %chosen_hbm.1, bf16[128,2048]{1,0:T(8,128)(2,1)} %queries.1, bf16[4,32,256]{2,1,0:T(8,128)(2,1)} %bitcast.5, bf16[4,32,256]{2,1,0:T(8,128)(2,1)} %bitcast.6, ...), custom_call_target="tpu_custom_call" | custom-call | tf_op jit(solution)/shard_map/attention_back/pallas_call | solution.py:598
  47.9 1.2 %write_out.1 = (f32[128,2048]{1,0:T(8,128)}, f32[4,32,256]{2,1,0:T(8,128)}, f32[4,32,256]{2,1,0:T(8,128)}, f32[256,256]{1,0:T(8,128)}) custom-call(f32[128,2048]{1,0:T(8,128)S(1)} %get-tuple-element.12.refs_0_, f32[4,32,256]{2,1,0:T(8,128)S(1)} %get-tuple-element.13.refs_1_, f32[4,32,256]{2,1,0:T(8,128)S(1)} %get-tuple-element.14.refs_2_, ...), custom_call_target="tpu_custom_call" | custom-call | tf_op jit(solution)/shard_map/write_out/pallas_call | solution.py:659

commit v2 on v1

--- a/solution.py
+++ b/solution.py
@@ -40,10 +40,6 @@
         return carry
 
     lax.fori_loop(first, last, step, 0)
-
-
-def mark(name):
-    pass
 
 
 def kernel(
@@ -66,10 +62,11 @@
     logs,
     log2s,
     normed,
+    column,
     pool,
-    ask,
     asked,
     named,
+    named_in,
     give,
     back_v,
     back_k,
@@ -87,19 +84,15 @@
     delta,
     dq_acc,
     in_sem,
-    ask_send,
+    send_sem,
     ask_recv,
-    out_send,
+    col_recv,
     kv_recv,
     bv_recv,
     bk_recv,
-    via_send,
     via_recv,
-    norm_send,
     norm_recv,
-    swap_send,
     swap_recv,
-    lo_send,
     lo_recv,
 ):
     me = lax.axis_index("kv")
@@ -126,7 +119,6 @@
 
     barrier = pltpu.get_barrier_semaphore()
 
-    mark("greet")
 
     def greet(i):
         pl.semaphore_signal(barrier, inc=1, device_id={"kv": i}, device_id_type=MESH)
@@ -141,10 +133,11 @@
         [pltpu.make_async_copy(chosen_hbm, chosen, in_sem.at[0])],
         [pltpu.make_async_copy(normed_hbm, normed, in_sem.at[1])],
         [
-            pltpu.make_async_copy(ref, pool.at[pl.ds(n, kblocks), a], in_sem.at[2 + a])
+            pltpu.make_async_copy(ref.at[:, :, lanes[g]], column.at[z, g, a], in_sem.at[2])
             for a, ref in ((0, keys), (1, values))
+            for g in range(kv_heads)
         ],
-        [pltpu.make_async_copy(logsum, logs, in_sem.at[4])],
+        [pltpu.make_async_copy(logsum, logs, in_sem.at[3])],
     ]
     big = []
     for a, (src, dst) in enumerate(((queries, q_all), (out_grad, do_all))):
@@ -155,7 +148,7 @@
                     pltpu.make_async_copy(
                         src.at[:, at : at + HD],
                         dst.at[g, h * tok : (h + 1) * tok],
-                        in_sem.at[5 + a],
+                        in_sem.at[4 + a],
                     )
                 )
     for cs in ins:
@@ -164,7 +157,6 @@
     for cp in big:
         cp.start()
 
-    mark("ask")
     for q in range(row):
 
         @pl.when(q >= r)
@@ -189,11 +181,10 @@
             far_own = jnp.where(block - me * kblocks == lane, 0.0, far_own)
         missing.append(jnp.broadcast_to(far[:1], (QB, HD)))
         missing_own.append(jnp.broadcast_to(far_own[:1], (QB, HD)))
-    ask[...] = wanted
+    asked[me] = wanted[:1]
     pen[...] = jnp.concatenate(missing, axis=0).T
     pen_own[...] = jnp.concatenate(missing_own, axis=0).T
 
-    mark("turn")
     ins[1][0].wait()
     for m in range(normed.shape[1] // HD):
         turned = normed[:, m * HD : (m + 1) * HD].T
@@ -201,26 +192,42 @@
             at = m * HD + p
             norm_parts[at % rows // sub, at // rows] = turned[p : p + sub]
 
-    mark("barrier")
     pl.semaphore_wait(barrier, n + tp - 1)
 
     def place(i):
         return jnp.where(i // row == z, zs + i % row, i // row)
 
-    mark("asksend")
 
     def ask_copy(i):
-        return remote(ask, asked.at[me], ask_send.at[i], ask_recv.at[place_of_me(i)], {"kv": i})
+        return remote(
+            asked.at[me], asked.at[me], send_sem.at[0], ask_recv.at[place_of_me(i)], {"kv": i}
+        )
 
     def place_of_me(i):
         return jnp.where(i // row == z, zs + r, z)
 
-    loop(0, me, lambda i: ask_copy(i).start())
+    def column_copy(p, g, a):
+        at = column.at[p, g, a]
+        return remote(at, at, send_sem.at[1], col_recv.at[p, g, a], {"kv": me + row})
+
+    def climb(p, g, a):
+        @pl.when(z + 1 < zs)
+        def _():
+            column_copy(p, g, a).start()
+
+    for cp in ins[2]:
+        cp.wait()
+    for g in range(kv_heads):
+        for a in range(2):
+            climb(z, g, a)
+    for d in range(1, row):
+        ask_copy(z * row + (r + d) % row).start()
+    loop(0, z * row, lambda i: ask_copy(i).start())
 
     def via_copy(d, k):
         q = (col + d) % tp
         return remote(
-            norm_parts.at[q, k], norm_via.at[d, k], via_send.at[d], via_recv.at[d, k], {"tp": q}
+            norm_parts.at[q, k], norm_via.at[d, k], send_sem.at[2], via_recv.at[d, k], {"tp": q}
         )
 
     for d in range(1, tp):
@@ -231,7 +238,7 @@
         dest = t * per + k
         src = norm_parts.at[col, k] if d == 0 else norm_via.at[d, k]
         return remote(
-            src, norm_pool.at[col, me], norm_send.at[0], norm_recv.at[place_of_me(dest)],
+            src, norm_pool.at[col, me], send_sem.at[3], norm_recv.at[place_of_me(dest)],
             {"kv": dest},
         )
 
@@ -255,11 +262,7 @@
             def _():
                 norm_copy(d, k).start()
 
-    mark("normlow")
-    loop(0, per, lambda k: norm_start(0, k, True))
-
-    mark("own")
-    for cp in ins[2] + ins[3]:
+    for cp in ins[3]:
         cp.wait()
     for cp in big:
         cp.wait()
@@ -269,16 +272,18 @@
         )
 
     def take(a, first, count, g):
-        return pool[pl.ds(first, count), a, :, lanes[g]].reshape(count * KB, HD)
+        if first is None:
+            return column[z, g, a].reshape(count * KB, HD)
+        return pool[pl.ds(first, count), g, a].reshape(count * KB, HD)
 
     key_iota = lax.broadcasted_iota(jnp.int32, (KB, tok), 0)
     row_iota = lax.broadcasted_iota(jnp.int32, (KB, tok), 1)
 
     def early(first, count, own):
         for g in range(kv_heads):
-            s_buf[: count * KB] = dot(take(0, first, count, g), q_all[g], ((1,), (1,)))
+            s_buf[: count * KB] = dot(take(0, None if own else first, count, g), q_all[g], ((1,), (1,)))
             dp[g, pl.ds(first, count)] = dot(
-                take(1, first, count, g), do_all[g], ((1,), (1,))
+                take(1, None if own else first, count, g), do_all[g], ((1,), (1,))
             ).reshape(count, KB, width)
             total = jnp.zeros((8, width), F32) if own else delta[g]
             for u in range(count):
@@ -303,31 +308,13 @@
 
     early(n, kblocks, True)
 
-    mark("answer")
-
-    def name(j):
-        mine = jnp.where(lane == me, asked[j], 0.0)
-        named[j] = jnp.broadcast_to(jnp.sum(mine, axis=1, keepdims=True), (8, kv_cols))
-
-    def masks(j):
-        return [
-            jnp.concatenate([named[j] == w + 1.0] * (KB // 8), axis=0) for w in range(kblocks)
-        ]
-
-    def kv_copy(j):
-        return remote(
-            give.at[j], pool.at[me], out_send.at[0], kv_recv.at[place_of_me(j)], {"kv": j}
-        )
-
-    def answer(j):
-        name(j)
-        hit = masks(j)
-        for a in range(2):
-            block = jnp.zeros((KB, kv_cols), F32)
-            for w in range(kblocks):
-                block = jnp.where(hit[w], pool[n + w, a].astype(F32), block)
-            give[j, a] = block.astype(BF16)
-        kv_copy(j).start()
+
+    def spell(v, at):
+        mine = jnp.where(lane == at, jnp.broadcast_to(v, (8, HD)), 0.0)
+        return jnp.broadcast_to(jnp.sum(mine, axis=1, keepdims=True), (8, HD))
+
+    def masks(v):
+        return [jnp.concatenate([v == w + 1.0] * (KB // 8), axis=0) for w in range(kblocks)]
 
     def wait_plane(ref, sem, k):
         at = ref.at[pl.ds(k * row, row)]
@@ -337,65 +324,116 @@
         at = ref.at[z * row + q]
         pltpu.make_async_copy(at, at, sem.at[zs + q]).wait()
 
-    def answer_plane(i):
-        k = zs - 1 - i
-        wait_plane(asked, ask_recv, k)
-        loop(0, row, lambda q: answer(k * row + q))
-
-    loop(0, zs - 1 - z, answer_plane)
-    for q in reversed(range(1, row)):
-
-        @pl.when(q > r)
+    def peers(act, test):
+        for q in range(row):
+
+            @pl.when(test(q))
+            def _():
+                act(q)
+
+    peers(lambda q: wait_peer(asked, ask_recv, q), lambda q: q != r)
+
+    def spell_plane(p):
+        for d in range(row):
+            named_in[p, d] = spell(asked[z * row + (r + d) % row], p * row + r)
+
+    loop(0, z + 1, spell_plane)
+
+    def give_copy(p, d):
+        return remote(
+            give.at[p, d],
+            pool.at[p * row + r],
+            send_sem.at[4],
+            kv_recv.at[p, r],
+            {"kv": z * row + (r + d) % row},
+        )
+
+    def pick(p, d, g, a, hit):
+        block = jnp.zeros((KB, HD), F32)
+        for w in range(kblocks):
+            block = jnp.where(hit[w], column[p, g, a, w].astype(F32), block)
+        return block.astype(BF16)
+
+    def answer(p, d):
+        hit = masks(named_in[p, d])
+        for g in range(kv_heads):
+            for a in range(2):
+                block = pick(p, d, g, a, hit)
+                if d == 0:
+                    pool[p * row + r, g, a] = block
+                else:
+                    give[p, d, g, a] = block
+        if d > 0:
+            give_copy(p, d).start()
+
+    for d in range(1, row):
+
+        @pl.when(r + d < row)
         def _():
-            wait_peer(asked, ask_recv, q)
-            answer(z * row + q)
-
-    mark("norm")
-    for d in range(1, tp):
-
-        def forward(k):
+            answer(z, d)
+
+    def bv_copy(i):
+        return remote(
+            back_v.at[i], got_v.at[me], send_sem.at[5], bv_recv.at[place_of_me(i)], {"kv": i}
+        )
+
+    def bk_copy(i):
+        return remote(
+            back_k.at[i], got_k.at[me], send_sem.at[6], bk_recv.at[place_of_me(i)], {"kv": i}
+        )
+
+    def wait_give(p, q):
+        at = pool.at[p * row + q]
+        pltpu.make_async_copy(at, at, kv_recv.at[p, q]).wait()
+
+    def near():
+        peers(lambda q: wait_give(z, q), lambda q: q < r)
+        early(z * row, row, False)
+        peers(lambda q: bv_copy(z * row + q).start(), lambda q: q < r)
+
+    def far(p):
+        peers(lambda q: wait_give(p, q), lambda q: q != r)
+        early(p * row, row, False)
+        loop(0, row, lambda q: bv_copy(p * row + q).start())
+
+    def forward(k):
+        for d in range(1, tp):
             at = norm_via.at[d, k]
             pltpu.make_async_copy(at, at, via_recv.at[d, k]).wait()
             norm_start(d, k, True)
 
-        loop(0, per, forward)
-    for d in range(tp):
-        loop(0, per, lambda k: norm_start(d, k, False))
-
-    mark("near")
-
-    def bv_copy(i):
-        return remote(
-            back_v.at[i], got_v.at[me], out_send.at[0], bv_recv.at[place_of_me(i)], {"kv": i}
-        )
-
-    def bk_copy(i):
-        return remote(
-            back_k.at[i], got_k.at[me], out_send.at[0], bk_recv.at[place_of_me(i)], {"kv": i}
-        )
-
-    def peers(act, test):
-        for q in range(row):
-
-            @pl.when(test(q))
-            def _():
-                act(q)
-
-    peers(lambda q: wait_peer(pool, kv_recv, q), lambda q: q < r)
-    early(z * row, row, False)
-    peers(lambda q: bv_copy(z * row + q).start(), lambda q: q < r)
-
-    mark("far")
-
-    def early_plane(i):
-        k = z - 1 - i
-        wait_plane(pool, kv_recv, k)
-        early(k * row, row, False)
-        loop(0, row, lambda q: bv_copy(k * row + q).start())
-
-    loop(0, z, early_plane)
-
-    mark("late")
+    share = per // 2
+    loop(0, per, lambda k: norm_start(0, k, True))
+
+    def descend(i):
+        p = z - 1 - i
+        for g in range(kv_heads):
+            for a in range(2):
+                at = column.at[p, g, a]
+                pltpu.make_async_copy(at, at, col_recv.at[p, g, a]).wait()
+                climb(p, g, a)
+        for d in reversed(range(row)):
+            answer(p, d)
+        loop(jnp.minimum(i, 2) * share, jnp.minimum(i + 1, 2) * share, forward)
+
+        @pl.when(i == 0)
+        def _():
+            near()
+
+        @pl.when(i > 0)
+        def _():
+            far(p + 1)
+
+    loop(0, z, descend)
+
+    @pl.when(z == 0)
+    def _():
+        near()
+
+    @pl.when(z > 0)
+    def _():
+        far(0)
+
     for g in range(kv_heads):
         delta[g] = jnp.broadcast_to(jnp.sum(delta[g], axis=0, keepdims=True), (8, width))
 
@@ -410,7 +448,7 @@
                 key_grad[:, :, lanes[g]] = dk
             else:
                 back_k[pl.ds(first, count), :, lanes[g]] = dk.astype(BF16)
-            dq = dot(take(0, first, count, g), ds, ((0,), (0,)))
+            dq = dot(take(0, None if own else first, count, g), ds, ((0,), (0,)))
             dq_acc[g] = dq if own else dq_acc[g] + dq
 
     late(n, kblocks, True)
@@ -418,21 +456,19 @@
     def late_plane(i):
         k = z - 1 - i
         late(k * row, row, False)
-        loop(0, row, lambda q: bk_copy(k * row + q).start())
 
     loop(0, z, late_plane)
     late(z * row, row, False)
-    peers(lambda q: bk_copy(z * row + q).start(), lambda q: q < r)
-
-    mark("dq")
+
     for g in range(kv_heads):
         for h in range(group):
             at = (g * group + h) * HD
             query_grad[:, at : at + HD] = dq_acc[g, :, h * tok : (h + 1) * tok].T * scale
 
+
     def swap_copy(d, k):
         at = norm_pool.at[col, pl.ds(k * row, row)]
-        return remote(at, at, swap_send.at[d], swap_recv.at[d, k], {"tp": (col + d) % tp})
+        return remote(at, at, send_sem.at[7], swap_recv.at[d, k], {"tp": (col + d) % tp})
 
     def swap(k):
         for d in range(1, tp):
@@ -442,91 +478,122 @@
         wait_plane(norm_pool.at[col], norm_recv, k)
         swap(k)
 
-    mark("swap1")
-    peers(lambda q: wait_peer(norm_pool.at[col], norm_recv, q), lambda q: q != r)
-    swap(z)
-    loop(z + 1, zs, swap_plane)
-
-    mark("addv")
+    loop(jnp.minimum(z, 2) * share, per, forward)
+    for d in range(tp):
+        loop(0, per, lambda k: norm_start(d, k, False))
+
+
+    def name(j):
+        named[j] = spell(asked[j], me)
+
+    def name_plane(k):
+        wait_plane(asked, ask_recv, k)
+        for q in range(row):
+            name(k * row + q)
+
+    for q in range(row):
+        name(z * row + q)
+    loop(z + 1, zs, name_plane)
+
 
     def add(j, got, out):
-        hit = masks(j)
+        hit = [jnp.concatenate([m] * kv_heads, axis=1) for m in masks(named[j])]
         term = got[j].astype(F32)
         for w in range(kblocks):
             out[w] += jnp.where(hit[w], term, 0.0)
 
-    def add_all(got, sem, out):
+    def add_near(got, sem, out):
         def one(q):
             wait_peer(got, sem, q)
             add(z * row + q, got, out)
 
         peers(one, lambda q: q > r)
 
+    def add_far(got, sem, out, first, last):
         def plane(k):
             wait_plane(got, sem, k)
             loop(0, row, lambda q: add(k * row + q, got, out))
 
-        loop(z + 1, zs, plane)
-
-    add_all(got_v, bv_recv, value_grad)
+        loop(first, last, plane)
+
+    add_near(got_v, bv_recv, value_grad)
+    above = jnp.minimum(z + 2, zs)
+    add_far(got_v, bv_recv, value_grad, z + 1, above)
+    add_far(got_v, bv_recv, value_grad, above, zs)
     low_pool[me] = value_grad[...].reshape(tok, kv_cols).astype(BF16)
 
-    mark("lowstart")
 
     def low_copy(slot, send, dest):
         return remote(
-            low_pool.at[slot], low_pool.at[slot], lo_send.at[send], lo_recv.at[slot], {"kv": dest}
+            low_pool.at[slot], low_pool.at[slot], send_sem.at[send], lo_recv.at[slot], {"kv": dest}
         )
 
     def low_wait(slot):
         at = low_pool.at[slot]
         pltpu.make_async_copy(at, at, lo_recv.at[slot]).wait()
 
-    def plane_of(k):
-        return (z - k + zs) % zs
-
-    loop(1, zs, lambda k: low_copy(me, 0, (z + k) % zs * row + r).start())
-
-    mark("swap2")
-    loop(0, z, swap_plane)
-
-    mark("lowrelay")
-
-    def slot_of(k, d, core):
-        return plane_of(k) * row + (x + d) % xs * 2 + core
-
-    def across(k, d):
-        low_copy(slot_of(k, d, c), 2, z * row + x * 2 + 1 - c).start()
-
-    def relay(k, first):
-        if not first:
-            low_wait(slot_of(k, 0, c))
+    def up(k):
+        return low_copy(me, 8, k * row + r)
+
+    def down(p):
+        return low_copy(p * row + r, 9, (z - 1) * row + r)
+
+    loop(0, zs - 1 - z, lambda i: up(zs - 1 - i).start())
+
+    @pl.when(z > 0)
+    def _():
+        down(z).start()
+
+
+    def slot_of(p, d, core):
+        return p * row + (x + d) % xs * 2 + core
+
+    def across(p, d):
+        low_copy(slot_of(p, d, c), 10, z * row + x * 2 + 1 - c).start()
+
+    def spread(p):
         for d in range(1, xs):
-            low_copy(slot_of(k, 0, c), 1, z * row + (x + d) % xs * 2 + c).start()
-        across(k, 0)
-
-    def cross(k):
+            low_copy(slot_of(p, 0, c), 11, z * row + (x + d) % xs * 2 + c).start()
+        across(p, 0)
+
+    def cross(p):
         for d in range(1, xs):
-            low_wait(slot_of(k, d, c))
-            across(k, d)
-
-    def relay_next(k):
-        relay(k, False)
-        cross(k - 1)
-
-    relay(0, True)
-    loop(1, zs, relay_next)
-    cross(zs - 1)
-
-    mark("addk")
-    add_all(got_k, bk_recv, key_grad)
-
-    mark("product")
+            low_wait(slot_of(p, d, c))
+            across(p, d)
+
+    def order(k):
+        return jnp.where(k < zs - z, z + k, zs - 1 - k)
+
+    spread(z)
+    peers(lambda q: wait_peer(norm_pool.at[col], norm_recv, q), lambda q: q != r)
+    swap(z)
+
+    def relay(k):
+        p = order(k)
+        slot = slot_of(p, 0, c)
+        swap_plane(p)
+        low_wait(slot)
+
+        @pl.when((p > z) & (z > 0))
+        def _():
+            down(p).start()
+
+        spread(p)
+        cross(order(k - 1))
+
+    relay(1)
+    loop(0, me, lambda i: bk_copy(i).start())
+    loop(2, zs, relay)
+    cross(order(zs - 1))
+
+    add_near(got_k, bk_recv, key_grad)
+    add_far(got_k, bk_recv, key_grad, z + 1, zs)
+
 
     def product(k, first):
-        p = plane_of(k)
+        p = order(k)
         for d in range(xs):
-            low_wait(slot_of(k, d, 1 - c))
+            low_wait(slot_of(p, d, 1 - c))
         for d in range(1, tp):
             q = (col + tp - d) % tp
             at = norm_pool.at[q, pl.ds(p * row, row)]
@@ -543,21 +610,49 @@
     product(0, True)
     loop(1, zs, lambda k: product(k, False))
 
-    mark("drain")
 
     def drain(ref, sem):
         pltpu.make_async_copy(ref, ref, sem).wait()
 
-    drain(low_pool.at[pl.ds(0, zs - 1)], lo_send.at[0])
-    drain(low_pool.at[pl.ds(0, zs * (xs - 1))], lo_send.at[1])
-    drain(low_pool.at[pl.ds(0, zs * xs)], lo_send.at[2])
-    drain(give.at[pl.ds(0, n - 1)], out_send.at[0])
-    drain(norm_pool.at[0, pl.ds(0, n - 1)], norm_send.at[0])
+    drain(low_pool.at[pl.ds(0, zs * xs)], send_sem.at[10])
+    drain(low_pool.at[pl.ds(0, zs * (xs - 1))], send_sem.at[11])
+    drain(norm_pool.at[0, pl.ds(0, n - 1)], send_sem.at[3])
     for d in range(1, tp):
-        drain(norm_parts.at[0], via_send.at[d])
-        drain(norm_pool.at[0], swap_send.at[d])
-    loop(0, me, lambda i: ask_copy(i).wait_send())
-    mark(None)
+        drain(norm_parts.at[0], send_sem.at[2])
+        drain(norm_pool.at[0], send_sem.at[7])
+    loop(z + 1, zs, lambda k: up(k).wait_send())
+
+    @pl.when(z > 0)
+    def _():
+        loop(z, zs, lambda p: down(p).wait_send())
+
+    for d in range(1, row):
+        ask_copy(z * row + (r + d) % row).wait_send()
+
+        @pl.when(r + d < row)
+        def _():
+            give_copy(z, d).wait_send()
+
+    def drain_plane(p):
+        for d in range(1, row):
+            give_copy(p, d).wait_send()
+
+    def drain_column(p):
+        for g in range(kv_heads):
+            for a in range(2):
+                column_copy(p, g, a).wait_send()
+
+    def drain_back(i):
+        bv_copy(i).wait_send()
+        bk_copy(i).wait_send()
+
+    loop(0, z, drain_plane)
+    loop(0, z * row, lambda i: ask_copy(i).wait_send())
+    loop(0, me, drain_back)
+
+    @pl.when(z + 1 < zs)
+    def _():
+        loop(0, z + 1, drain_column)
 
 
 def finish(*refs):
@@ -607,11 +702,12 @@
             pltpu.VMEM((heads, tok), F32),
             pltpu.VMEM((kv_heads, 1, width), F32),
             pltpu.VMEM(normed_input.shape, BF16),
-            pltpu.VMEM((slots, 2, KB, kv_cols), BF16),
-            pltpu.VMEM((8, HD), F32),
+            pltpu.VMEM((zs, kv_heads, 2, kblocks, KB, HD), BF16),
+            pltpu.VMEM((n, kv_heads, 2, KB, HD), BF16),
+            pltpu.VMEM((n, 1, HD), F32),
             pltpu.VMEM((n, 8, HD), F32),
-            pltpu.VMEM((n, 8, kv_cols), F32),
-            pltpu.VMEM((n, 2, KB, kv_cols), BF16),
+            pltpu.VMEM((zs, row, 8, HD), F32),
+            pltpu.VMEM((zs, row, kv_heads, 2, KB, HD), BF16),
             pltpu.VMEM((n, KB, kv_cols), BF16),
             pltpu.VMEM((n, KB, kv_cols), BF16),
             pltpu.VMEM((n, KB, kv_cols), BF16),
@@ -627,20 +723,16 @@
             pltpu.VMEM((kv_heads, slots, KB, width), BF16),
             pltpu.VMEM((kv_heads, 8, width), F32),
             pltpu.VMEM((kv_heads, HD, width), F32),
-            dma((7,)),
-            dma((n,)),
+            dma((6,)),
+            dma((12,)),
             dma((groups,)),
-            dma((1,)),
+            dma((zs, kv_heads, 2)),
+            dma((zs, row)),
             dma((groups,)),
             dma((groups,)),
+            dma((tp, per)),
             dma((groups,)),
-            dma((tp,)),
-            dma((tp, per)),
-            dma((1,)),
-            dma((groups,)),
-            dma((tp,)),
             dma((tp, zs)),
-            dma((3,)),
             dma((n,)),
         ],
         compiler_params=pltpu.CompilerParams(

time: 49.7 us -> 46.7 us (0.940)
  Pallas kernels: 48.4 us -> 45.8 us
    pallas_call x1, Pallas kernels: 47.2 us -> 44.7 us  [local(): pl.pallas_call(functools.partial(kernel, n, tp), out_shape=tuple((pltpu.V...]
where the time goes in v2:
time: 46.7 us; the launch traced here: 46.5 us
  Pallas kernels  45.8 us (98%)
  between operations  0.64 us (1%)
    pallas_call x1, Pallas kernels, local(): pl.pallas_call(functools.partial(kernel, n, tp), out_shape=tuple((pltpu.V...  44.7 us
    pallas_call x1, Pallas kernels, local(): pl.pallas_call(finish, out_shape=tuple((jax.ShapeDtypeStruct(shape, F32)...  1.17 us

profile of v2, /device:TPU:0, one launch (start us, length us, event | category | flops | bytes accessed | tf_op | source)
XLA Modules:
  0.0 46.5 jit_solution(13043631752090103292)
XLA Ops:
  0.6 44.7 %attention_back.1 = (f32[128,2048]{1,0:T(8,128)S(1)}, f32[4,32,256]{2,1,0:T(8,128)S(1)}, f32[4,32,256]{2,1,0:T(8,128)S(1)}, f32[256,256]{1,0:T(8,128)S(1)}) custom-call(s32[2,16]{1,0:T(2,128)} %chosen_hbm.1, bf16[128,2048]{1,0:T(8,128)(2,1)} %queries.1, bf16[4,32,256]{2,1,0:T(8,128)(2,1)} %bitcast.5, bf16[4,32,256]{2,1,0:T(8,128)(2,1)} %bitcast.6, ...), custom_call_target="tpu_custom_call" | custom-call | tf_op jit(solution)/shard_map/attention_back/pallas_call | solution.py:693
  45.3 1.2 %write_out.1 = (f32[128,2048]{1,0:T(8,128)}, f32[4,32,256]{2,1,0:T(8,128)}, f32[4,32,256]{2,1,0:T(8,128)}, f32[256,256]{1,0:T(8,128)}) custom-call(f32[128,2048]{1,0:T(8,128)S(1)} %get-tuple-element.12.refs_0_, f32[4,32,256]{2,1,0:T(8,128)S(1)} %get-tuple-element.13.refs_1_, f32[4,32,256]{2,1,0:T(8,128)S(1)} %get-tuple-element.14.refs_2_, ...), custom_call_target="tpu_custom_call" | custom-call | tf_op jit(solution)/shard_map/write_out/pallas_call | solution.py:751

commit v3 on v2

--- a/solution.py
+++ b/solution.py
@@ -12,6 +12,9 @@
 KB = 32
 NSEL = 16
 FAR = 1e30
+EARLY2 = 8
+EARLY = 6
+EARLY1 = 4
 LOG2E = 1.4426950408889634
 
 MESH = pl.DeviceIdType.MESH
@@ -148,7 +151,7 @@
                     pltpu.make_async_copy(
                         src.at[:, at : at + HD],
                         dst.at[g, h * tok : (h + 1) * tok],
-                        in_sem.at[4 + a],
+                        in_sem.at[3],
                     )
                 )
     for cs in ins:
@@ -208,7 +211,7 @@
 
     def column_copy(p, g, a):
         at = column.at[p, g, a]
-        return remote(at, at, send_sem.at[1], col_recv.at[p, g, a], {"kv": me + row})
+        return remote(at, at, send_sem.at[0], col_recv.at[p, g, a], {"kv": me + row})
 
     def climb(p, g, a):
         @pl.when(z + 1 < zs)
@@ -227,7 +230,7 @@
     def via_copy(d, k):
         q = (col + d) % tp
         return remote(
-            norm_parts.at[q, k], norm_via.at[d, k], send_sem.at[2], via_recv.at[d, k], {"tp": q}
+            norm_parts.at[q, k], norm_via.at[d, k], send_sem.at[0], via_recv.at[d - 1, k], {"tp": q}
         )
 
     for d in range(1, tp):
@@ -238,7 +241,7 @@
         dest = t * per + k
         src = norm_parts.at[col, k] if d == 0 else norm_via.at[d, k]
         return remote(
-            src, norm_pool.at[col, me], send_sem.at[3], norm_recv.at[place_of_me(dest)],
+            src, norm_pool.at[col, me], send_sem.at[0], norm_recv.at[place_of_me(dest)],
             {"kv": dest},
         )
 
@@ -343,7 +346,7 @@
         return remote(
             give.at[p, d],
             pool.at[p * row + r],
-            send_sem.at[4],
+            send_sem.at[0],
             kv_recv.at[p, r],
             {"kv": z * row + (r + d) % row},
         )
@@ -374,12 +377,12 @@
 
     def bv_copy(i):
         return remote(
-            back_v.at[i], got_v.at[me], send_sem.at[5], bv_recv.at[place_of_me(i)], {"kv": i}
+            back_v.at[i], got_v.at[me], send_sem.at[0], bv_recv.at[place_of_me(i)], {"kv": i}
         )
 
     def bk_copy(i):
         return remote(
-            back_k.at[i], got_k.at[me], send_sem.at[6], bk_recv.at[place_of_me(i)], {"kv": i}
+            back_k.at[i], got_k.at[me], send_sem.at[0], bk_recv.at[place_of_me(i)], {"kv": i}
         )
 
     def wait_give(p, q):
@@ -399,11 +402,21 @@
     def forward(k):
         for d in range(1, tp):
             at = norm_via.at[d, k]
-            pltpu.make_async_copy(at, at, via_recv.at[d, k]).wait()
-            norm_start(d, k, True)
-
-    share = per // 2
-    loop(0, per, lambda k: norm_start(0, k, True))
+            pltpu.make_async_copy(at, at, via_recv.at[d - 1, k]).wait()
+
+            @pl.when(k < share)
+            def _():
+                norm_start(d, k, True)
+
+    soon = jnp.where(col == 0, per * EARLY // 8, per * EARLY1 // 8)
+    soon2 = per * EARLY2 // 8
+    share = jnp.where(z == zs - 1, soon, jnp.where(z == zs - 2, soon2, per))
+    half = per // 2
+
+    def begin(i):
+        return jnp.minimum(i, 2) * half
+
+    loop(0, share, lambda k: norm_start(0, k, True))
 
     def descend(i):
         p = z - 1 - i
@@ -414,7 +427,7 @@
                 climb(p, g, a)
         for d in reversed(range(row)):
             answer(p, d)
-        loop(jnp.minimum(i, 2) * share, jnp.minimum(i + 1, 2) * share, forward)
+        loop(begin(i), begin(i + 1), forward)
 
         @pl.when(i == 0)
         def _():
@@ -425,6 +438,15 @@
             far(p + 1)
 
     loop(0, z, descend)
+    steep = (z == zs - 2) & (z > 0)
+
+    def norm_up():
+        for d in range(tp):
+            loop(0, per, lambda k: norm_start(d, k, False))
+
+    @pl.when(steep)
+    def _():
+        norm_up()
 
     @pl.when(z == 0)
     def _():
@@ -433,9 +455,6 @@
     @pl.when(z > 0)
     def _():
         far(0)
-
-    for g in range(kv_heads):
-        delta[g] = jnp.broadcast_to(jnp.sum(delta[g], axis=0, keepdims=True), (8, width))
 
     def late(first, count, own):
         for g in range(kv_heads):
@@ -451,24 +470,13 @@
             dq = dot(take(0, None if own else first, count, g), ds, ((0,), (0,)))
             dq_acc[g] = dq if own else dq_acc[g] + dq
 
-    late(n, kblocks, True)
-
     def late_plane(i):
         k = z - 1 - i
         late(k * row, row, False)
 
-    loop(0, z, late_plane)
-    late(z * row, row, False)
-
-    for g in range(kv_heads):
-        for h in range(group):
-            at = (g * group + h) * HD
-            query_grad[:, at : at + HD] = dq_acc[g, :, h * tok : (h + 1) * tok].T * scale
-
-
     def swap_copy(d, k):
         at = norm_pool.at[col, pl.ds(k * row, row)]
-        return remote(at, at, send_sem.at[7], swap_recv.at[d, k], {"tp": (col + d) % tp})
+        return remote(at, at, send_sem.at[0], swap_recv.at[d - 1, k], {"tp": (col + d) % tp})
 
     def swap(k):
         for d in range(1, tp):
@@ -477,11 +485,6 @@
     def swap_plane(k):
         wait_plane(norm_pool.at[col], norm_recv, k)
         swap(k)
-
-    loop(jnp.minimum(z, 2) * share, per, forward)
-    for d in range(tp):
-        loop(0, per, lambda k: norm_start(d, k, False))
-
 
     def name(j):
         named[j] = spell(asked[j], me)
@@ -490,11 +493,6 @@
         wait_plane(asked, ask_recv, k)
         for q in range(row):
             name(k * row + q)
-
-    for q in range(row):
-        name(z * row + q)
-    loop(z + 1, zs, name_plane)
-
 
     def add(j, got, out):
         hit = [jnp.concatenate([m] * kv_heads, axis=1) for m in masks(named[j])]
@@ -516,16 +514,16 @@
 
         loop(first, last, plane)
 
-    add_near(got_v, bv_recv, value_grad)
-    above = jnp.minimum(z + 2, zs)
-    add_far(got_v, bv_recv, value_grad, z + 1, above)
-    add_far(got_v, bv_recv, value_grad, above, zs)
-    low_pool[me] = value_grad[...].reshape(tok, kv_cols).astype(BF16)
-
-
+    def swap_own():
+        peers(lambda q: wait_peer(norm_pool.at[col], norm_recv, q), lambda q: q != r)
+        swap(z)
+
+    at = me % per
+    ready = jnp.where(at >= soon2, zs - 2, jnp.where(at >= soon, zs - 1, zs))
+    ready = jnp.maximum(jnp.minimum(ready, zs), z + 1)
     def low_copy(slot, send, dest):
         return remote(
-            low_pool.at[slot], low_pool.at[slot], send_sem.at[send], lo_recv.at[slot], {"kv": dest}
+            low_pool.at[slot], low_pool.at[slot], send_sem.at[0], lo_recv.at[slot], {"kv": dest}
         )
 
     def low_wait(slot):
@@ -537,12 +535,6 @@
 
     def down(p):
         return low_copy(p * row + r, 9, (z - 1) * row + r)
-
-    loop(0, zs - 1 - z, lambda i: up(zs - 1 - i).start())
-
-    @pl.when(z > 0)
-    def _():
-        down(z).start()
 
 
     def slot_of(p, d, core):
@@ -564,14 +556,70 @@
     def order(k):
         return jnp.where(k < zs - z, z + k, zs - 1 - k)
 
-    spread(z)
-    peers(lambda q: wait_peer(norm_pool.at[col], norm_recv, q), lambda q: q != r)
-    swap(z)
+    def finish_keys():
+        for g in range(kv_heads):
+            total = jnp.sum(delta[g], axis=0, keepdims=True)
+            delta[g] = jnp.broadcast_to(total, (8, width))
+        late(n, kblocks, True)
+        loop(0, z, late_plane)
+        late(z * row, row, False)
+        for g in range(kv_heads):
+            for h in range(group):
+                at = (g * group + h) * HD
+                query_grad[:, at : at + HD] = dq_acc[g, :, h * tok : (h + 1) * tok].T * scale
+        loop(begin(z), per, forward)
+        for d in range(tp):
+            loop(share, per, lambda k: norm_start(d, k, True))
+
+        @pl.when(jnp.logical_not(steep))
+        def _():
+            norm_up()
+
+    def finish_values():
+        for q in range(row):
+            name(z * row + q)
+        loop(z + 1, zs, name_plane)
+        @pl.when(z < zs - 1)
+        def _():
+            swap_own()
+        loop(z + 1, ready, swap_plane)
+        add_near(got_v, bv_recv, value_grad)
+        above = jnp.minimum(z + 2, zs)
+        add_far(got_v, bv_recv, value_grad, z + 1, above)
+        add_far(got_v, bv_recv, value_grad, above, zs)
+        low_pool[me] = value_grad[...].reshape(tok, kv_cols).astype(BF16)
+        loop(0, zs - 1 - z, lambda i: up(zs - 1 - i).start())
+
+        @pl.when(z > 0)
+        def _():
+            down(z).start()
+        spread(z)
+
+    turn = jnp.where(z >= zs - 2, 0, 1)
+
+    def finish_both(i):
+        @pl.when(i == turn)
+        def _():
+            finish_values()
+
+        @pl.when(i == 1 - turn)
+        def _():
+            finish_keys()
+
+    loop(0, 2, finish_both)
+
+    @pl.when(z == zs - 1)
+    def _():
+        swap_own()
 
     def relay(k):
         p = order(k)
         slot = slot_of(p, 0, c)
-        swap_plane(p)
+
+        @pl.when(p < z)
+        def _():
+            swap_plane(p)
+
         low_wait(slot)
 
         @pl.when((p > z) & (z > 0))
@@ -579,16 +627,6 @@
             down(p).start()
 
         spread(p)
-        cross(order(k - 1))
-
-    relay(1)
-    loop(0, me, lambda i: bk_copy(i).start())
-    loop(2, zs, relay)
-    cross(order(zs - 1))
-
-    add_near(got_k, bk_recv, key_grad)
-    add_far(got_k, bk_recv, key_grad, z + 1, zs)
-
 
     def product(k, first):
         p = order(k)
@@ -597,7 +635,7 @@
         for d in range(1, tp):
             q = (col + tp - d) % tp
             at = norm_pool.at[q, pl.ds(p * row, row)]
-            pltpu.make_async_copy(at, at, swap_recv.at[d, p]).wait()
+            pltpu.make_async_copy(at, at, swap_recv.at[d - 1, p]).wait()
         v = low_pool[pl.ds(p * row, row)].reshape(row * tok, kv_cols)
         for q in range(tp):
             a = jnp.concatenate([norm_pool[q, p * row + i] for i in range(row)], axis=1)
@@ -607,19 +645,36 @@
             else:
                 weight_grad[q * sub : (q + 1) * sub] += w
 
+    for k in range(1, zs):
+        relay(k)
+        if k > 1:
+            cross(order(k - 2))
+        if k == 1:
+            loop(0, me, lambda i: bk_copy(i).start())
+
+        if k == 1:
+            loop(ready, zs, swap_plane)
+
     product(0, True)
-    loop(1, zs, lambda k: product(k, False))
+    cross(order(zs - 2))
+    for k in range(1, zs - 2):
+        product(k, False)
+    cross(order(zs - 1))
+    add_near(got_k, bk_recv, key_grad)
+    add_far(got_k, bk_recv, key_grad, z + 1, zs)
+    for k in range(max(zs - 2, 1), zs):
+        product(k, False)
 
 
     def drain(ref, sem):
         pltpu.make_async_copy(ref, ref, sem).wait()
 
-    drain(low_pool.at[pl.ds(0, zs * xs)], send_sem.at[10])
-    drain(low_pool.at[pl.ds(0, zs * (xs - 1))], send_sem.at[11])
-    drain(norm_pool.at[0, pl.ds(0, n - 1)], send_sem.at[3])
+    drain(low_pool.at[pl.ds(0, zs * xs)], send_sem.at[0])
+    drain(low_pool.at[pl.ds(0, zs * (xs - 1))], send_sem.at[0])
+    drain(norm_pool.at[0, pl.ds(0, n - 1)], send_sem.at[0])
     for d in range(1, tp):
-        drain(norm_parts.at[0], send_sem.at[2])
-        drain(norm_pool.at[0], send_sem.at[7])
+        drain(norm_parts.at[0], send_sem.at[0])
+        drain(norm_pool.at[0], send_sem.at[0])
     loop(z + 1, zs, lambda k: up(k).wait_send())
 
     @pl.when(z > 0)
@@ -723,16 +778,16 @@
             pltpu.VMEM((kv_heads, slots, KB, width), BF16),
             pltpu.VMEM((kv_heads, 8, width), F32),
             pltpu.VMEM((kv_heads, HD, width), F32),
-            dma((6,)),
-            dma((12,)),
+            dma((4,)),
+            dma((1,)),
             dma((groups,)),
             dma((zs, kv_heads, 2)),
             dma((zs, row)),
             dma((groups,)),
             dma((groups,)),
-            dma((tp, per)),
+            dma((tp - 1, per)),
             dma((groups,)),
-            dma((tp, zs)),
+            dma((tp - 1, zs)),
             dma((n,)),
         ],
         compiler_params=pltpu.CompilerParams(

time: 46.7 us -> 44.7 us (0.957); the launches traced: 46.5 us -> 43.9 us
  Pallas kernels: 45.8 us -> 43.3 us
    pallas_call x1, Pallas kernels: 44.7 us -> 42.1 us  [local(): pl.pallas_call(functools.partial(kernel, n, tp), out_shape=tuple((pltpu.V...]
where the time goes in v3:
time: 44.7 us; the launch traced here: 43.9 us
  Pallas kernels  43.3 us (97%)
  between operations  0.64 us (1%)
    pallas_call x1, Pallas kernels, local(): pl.pallas_call(functools.partial(kernel, n, tp), out_shape=tuple((pltpu.V...  42.1 us
    pallas_call x1, Pallas kernels, local(): pl.pallas_call(finish, out_shape=tuple((jax.ShapeDtypeStruct(shape, F32)...  1.17 us

profile of v3, /device:TPU:0, one launch (start us, length us, event | category | flops | bytes accessed | tf_op | source)
XLA Modules:
  0.0 43.9 jit_solution(3865450630612587395)
XLA Ops:
  0.6 42.1 %attention_back.1 = (f32[128,2048]{1,0:T(8,128)S(1)}, f32[4,32,256]{2,1,0:T(8,128)S(1)}, f32[4,32,256]{2,1,0:T(8,128)S(1)}, f32[256,256]{1,0:T(8,128)S(1)}) custom-call(s32[2,16]{1,0:T(2,128)} %chosen_hbm.1, bf16[128,2048]{1,0:T(8,128)(2,1)} %queries.1, bf16[4,32,256]{2,1,0:T(8,128)(2,1)} %bitcast.5, bf16[4,32,256]{2,1,0:T(8,128)(2,1)} %bitcast.6, ...), custom_call_target="tpu_custom_call" | custom-call | tf_op jit(solution)/shard_map/attention_back/pallas_call | solution.py:748
  42.8 1.2 %write_out.1 = (f32[128,2048]{1,0:T(8,128)}, f32[4,32,256]{2,1,0:T(8,128)}, f32[4,32,256]{2,1,0:T(8,128)}, f32[256,256]{1,0:T(8,128)}) custom-call(f32[128,2048]{1,0:T(8,128)S(1)} %get-tuple-element.12.refs_0_, f32[4,32,256]{2,1,0:T(8,128)S(1)} %get-tuple-element.13.refs_1_, f32[4,32,256]{2,1,0:T(8,128)S(1)} %get-tuple-element.14.refs_2_, ...), custom_call_target="tpu_custom_call" | custom-call | tf_op jit(solution)/shard_map/write_out/pallas_call | solution.py:806
